TPU v7x, 512 devices: a whole 4x4x16 slice. The times are simulated.
512 devices in a mesh: sp: 16 (over z), fs: 4 (over y), tp: 8 (over x, core).
Axes of the slice: x: 4, y: 4, z: 16, core: 2. Of those that a mesh axis runs over, the one named last changes fastest.
Arguments:
- tokens: bfloat16 [4, 4096, 2048], P('fs', 'sp'), may hold values from -6 to 6
- norm_gain: float32 [2048], replicated, may hold values from 0.1 to 1.9
- w_state_in: bfloat16 [2048, 1024], P(('sp', 'fs'), 'tp'), may hold values from -0.125 to 0.125
- w_value: bfloat16 [2048, 1024], P(('sp', 'fs'), 'tp'), may hold values from -0.125 to 0.125
- w_outer: bfloat16 [2048, 1024], P(('sp', 'fs'), 'tp'), may hold values from -0.125 to 0.125
- w_inner: bfloat16 [2048, 1024], P(('sp', 'fs'), 'tp'), may hold values from -0.125 to 0.125
- w_state_out: bfloat16 [2048, 1024], P(('sp', 'fs'), 'tp'), may hold values from -0.125 to 0.125
- w_conv_out: bfloat16 [2048, 1024], P(('sp', 'fs'), 'tp'), may hold values from -0.125 to 0.125
- log_step: float32 [64], P('tp'), may hold values from -4.6 to -3.2
- decay_real: float32 [64, 64], P('tp'), may hold values from -5 to 0
- frequency: float32 [64, 64], P('tp'), may hold values from 1 to 192
- step_rate: float32 [4, 4096], P('fs', 'sp'), may hold values from 0.4 to 2.5
- input_real: float32 [64, 64, 16], P('tp'), may hold values from -1 to 1
- input_imag: float32 [64, 64, 16], P('tp'), may hold values from -1 to 1
- read_real: float32 [64, 16, 64], P('tp'), may hold values from -0.75 to 0.75
- read_imag: float32 [64, 16, 64], P('tp'), may hold values from -0.75 to 0.75
- skip_gain: float32 [64, 16], P('tp'), may hold values from -4 to 4
- conv_taps: float32 [3, 1024], P(None, 'tp'), may hold values from -3.5 to 3.5
- initial_state: float32 [4, 2, 64, 64], P('fs', None, 'tp'), may hold values from -6 to 6
Outputs:
- mixed: bfloat16 [4, 4096, 2048], P('fs', ('sp', 'tp'))
- final_state: float32 [4, 2, 64, 64], P('fs', None, 'tp', 'sp')
All inputs are finite; a program needn't handle non-finite values.
Results may differ from a plain program's by a relative error of at most 0.018.
Values may be sent and summed in bfloat16 or wider, within the bound.
A program may use at most 64 MiB of HBM per device.

v0:
```python
import math

import jax
import jax.numpy as jnp
from jax import lax
from jax.experimental import pallas as pl
from jax.experimental.pallas import tpu as pltpu
from jax.sharding import PartitionSpec as P

MESH = pl.DeviceIdType.MESH
HIGHEST = lax.Precision.HIGHEST
F32, BF16 = jnp.float32, jnp.bfloat16
NZ, NY, NX = 16, 4, 4
ROWS, D, CH, FLAT = 256, 2048, 128, 512
NT = (((1,), (1,)), ((), ()))
NCHUNK = 4
CW = D // NCHUNK
NEAR = 5
FAR_FIRST = (8, 7, 9, 6, 10, 5, 11, 4, 12, 3, 13, 2, 14, 1, 15)
SIN = [math.pi, -(math.pi**3) / 6, math.pi**5 / 120, -(math.pi**7) / 5040, math.pi**9 / 362880, -(math.pi**11) / 39916800]
COS = [1.0, -(math.pi**2) / 2, math.pi**4 / 24, -(math.pi**6) / 720, math.pi**8 / 40320, -(math.pi**10) / 3628800, math.pi**12 / 479001600]


def horner(coefs, x):
    total = jnp.full_like(x, coefs[-1])
    for c in coefs[-2::-1]:
        total = total * x + c
    return total


def complex_power(rate, turn, fall):
    u = rate * turn
    r = u - jnp.round(u)
    x = r * r
    s = r * horner(SIN, x)
    c = horner(COS, x)
    grow = jnp.exp2(rate * fall)
    return grow * (1.0 - 2.0 * (s * s)), grow * (2.0 * (s * c))


def iota(shape, dim):
    return lax.broadcasted_iota(jnp.int32, shape, dim)


def lanes4(x):
    return jnp.concatenate([x, x, x, x], axis=1)


def layer_kernel(*refs):
    n_small = 12
    tokens = refs[0]
    shards = refs[1:7]
    small = refs[7 : 7 + n_small]
    out, fin = refs[7 + n_small : 9 + n_small]
    rest = refs[9 + n_small :]
    small_v = rest[:n_small]
    (
        wb, tk, nb, prm, pk, ratep, tchunk, ring_t, br, bi, pc, dr, di, coup, readw, xp_s, ext, ht,
        ends, ec, hc, rows8, hd, mix, ps, pr, cs, rl, rb,
        ssem, lsem, tsem, bz_s, bz_r, by_s, by_r, br_r, bw_r, tz_s, tz_r, h_s, h_r, e_s, e_r,
        p_s, p_r, x_s, x_r,
    ) = rest[n_small:]
    gain, lstep, decay, freq, rate, in_r, in_i, rd_r, rd_i, skip, taps, init = small_v
    z = lax.axis_index("sp")
    y = lax.axis_index("fs")
    t = lax.axis_index("tp")
    xx, cc = t // 2, lax.rem(t, 2)
    other = 1 - cc
    zn = lax.rem(z + 1, NZ)

    barrier = pltpu.get_barrier_semaphore()
    for n in (z + 1, z + NZ - 1, z + 2, z + NZ - 2):
        pl.semaphore_signal(barrier, inc=1, device_id=(lax.rem(n, NZ), y, t), device_id_type=MESH)
    for d in range(1, NY):
        pl.semaphore_signal(barrier, inc=1, device_id=(z, lax.rem(y + d, NY), t), device_id_type=MESH)
    for d in (1, NX - 1):
        pl.semaphore_signal(barrier, inc=1, device_id=(z, y, lax.rem(xx + d, NX) * 2 + cc), device_id_type=MESH)
    pl.semaphore_signal(barrier, inc=1, device_id=(z, y, xx * 2 + other), device_id_type=MESH)

    loads = [pltpu.make_async_copy(s, v, ssem.at[n]) for n, (s, v) in enumerate(zip(small, small_v))]
    def take(ref, sem):
        pltpu.make_async_copy(ref, ref, sem).wait()

    local = [pltpu.make_async_copy(shards[w], wb.at[z, y, w], lsem) for w in range(6)]
    tok = pltpu.make_async_copy(tokens, tk, tsem)
    for c in local:
        c.start()
    for c in loads:
        c.start()
    tok.start()
    pl.semaphore_wait(barrier, 10)
    take(wb.at[0, 0], lsem)

    def at_distance(k, side):
        return lax.rem(z + (k if side else NZ - k), NZ)

    def of_part(rows, part):
        return rows.at[0] if part == 0 else rows.at[pl.ds(1, 3)] if part == 1 else rows.at[pl.ds(4, 2)]

    def b_z(part, k, side, hop):
        rows = of_part(wb.at[at_distance(k, side), y], part)
        return pltpu.make_async_remote_copy(
            rows, rows, bz_s, bz_r.at[part, side, k + hop - 1],
            device_id=(at_distance(hop, 1 - side), y, t), device_id_type=MESH)

    def w_y(k, side, d, came=0, further=False):
        zb = at_distance(k, side)
        rows = of_part(wb.at[zb, lax.rem(y - came + NY, NY)], 2)
        return pltpu.make_async_remote_copy(
            rows, rows, by_s, bw_r.at[zb] if further else by_r.at[3],
            device_id=(z, lax.rem(y + d, NY), t), device_id_type=MESH)

    def b_y(k, side, d, came=0, further=False):
        zb = at_distance(k, side)
        rows = wb.at[zb, lax.rem(y - came + NY, NY)]
        rows = rows.at[pl.ds(0, 4)] if k < NEAR else of_part(rows, 1)
        return pltpu.make_async_remote_copy(
            rows, rows, by_s, br_r.at[zb] if further else by_r.at[0 if k < NEAR else 2],
            device_id=(z, lax.rem(y + d, NY), t), device_id_type=MESH)

    def s_y(k, side, d):
        rows = wb.at[at_distance(k, side), y, 0]
        return pltpu.make_async_remote_copy(
            rows, rows, by_s, by_r.at[1], device_id=(z, lax.rem(y + d, NY), t), device_id_type=MESH)

    def t_copy(d):
        return pltpu.make_async_remote_copy(
            ring_t.at[z], ring_t.at[z], tz_s, tz_r, device_id=(lax.rem(z + d, NZ), y, t), device_id_type=MESH)

    for part in (0, 1, 2):
        for hop in (2, 1):
            for side in (0, 1):
                b_z(part, 0, side, hop).start()
    b_y(0, 0, 1, further=True).start()
    b_y(0, 0, 3).start()

    for c in loads:
        c.wait()
    row, col = iota((ROWS, ROWS), 0), iota((ROWS, ROWS), 1)
    interleave = col == (row & 7) * 32 + (row >> 3)
    spread = jnp.where(interleave, rate[...], 0.0)
    ratep[...] = jnp.dot(spread, jnp.ones((ROWS, 128), F32), precision=HIGHEST, preferred_element_type=F32)
    totals = jnp.sum(ratep[...].reshape(32, 8, 128), axis=0)
    tchunk[...] = totals
    ring_t[z] = jnp.sum(totals, axis=0, keepdims=True)

    h_copy = pltpu.make_async_remote_copy(
        tokens.at[pl.ds(ROWS - 8, 8), :], ht, h_s, h_r, device_id=(zn, y, t), device_id_type=MESH)
    h_copy.start()

    tall = jnp.concatenate([decay[...], freq[...], init[...]], axis=0)
    hot = ((iota((64, FLAT), 1) & 63) == iota((64, FLAT), 0)).astype(F32)
    wide = jnp.dot(tall, hot, precision=HIGHEST, preferred_element_type=F32)
    own = (iota((8, FLAT), 1) >> 6) == iota((8, FLAT), 0)

    def line(v):
        return jnp.sum(jnp.where(own, v, 0.0), axis=0, keepdims=True)

    decay_l, freq_l = line(wide[0:8]), line(wide[8:16])
    column = jnp.sum(jnp.where(iota((8, 8), 0) == iota((8, 8), 1), lstep[...], 0.0), axis=1, keepdims=True)
    dt = jnp.exp(line(jnp.broadcast_to(column, (8, FLAT))))
    modulus = decay_l * decay_l + freq_l * freq_l
    lines = [dt * freq_l * (0.5 / math.pi), dt * decay_l * math.log2(math.e), decay_l / modulus, -freq_l / modulus,
             line(wide[16:24]), line(wide[24:32])]
    for n, v in enumerate(lines):
        prm[n : n + 1, :] = v
        for i in range(4):
            pk[n, i : i + 1, :] = v[:, i * 128 : (i + 1) * 128]
    c_re, c_im = complex_power(lanes4(tchunk[...]), prm[0:1, :], prm[1:2, :])
    pc[0] = c_re
    pc[1] = c_im
    block_t = (iota((CH, FLAT), 1) >> 6) == (iota((CH, FLAT), 0) >> 4)
    hot64 = hot.astype(BF16)
    for n, (dst, src, sign) in enumerate(((coup, in_r, 1), (coup, in_i, 1), (readw, rd_r, 1), (readw, rd_i, -1))):
        w = jnp.dot(src[...].astype(BF16), hot64, preferred_element_type=F32)
        at = (n % 2) * FLAT
        dst[:, at : at + FLAT] = jnp.where(block_t, sign * w, 0.0).astype(BF16)
    tok.wait()

    def normalized(f):
        mean_square = jnp.mean(f * f, axis=-1, keepdims=True)
        return (f * lax.rsqrt(mean_square + 1e-06) * gain[...]).astype(BF16)

    def work(k):
        rows = pl.ds(pl.multiple_of((k - 1) * 32, 32), 32)
        nb[rows, :] = normalized(tk[rows, :].astype(F32))
        for half in range(2):
            rows = pl.ds(pl.multiple_of((k - 1) * 32 + half * 16, 16), 16)
            re, im = complex_power(lanes4(ratep[rows, :]), prm[0:1, :], prm[1:2, :])
            br[rows, :] = re
            bi[rows, :] = im

    def sides_of(k):
        return (0, 1) if 0 < k < 8 else (0,)

    def step_w(k):
        for s in sides_of(k):
            b_z(2, k - 1, s, 1).wait_recv()
            if k + 2 <= (7 if s else 8):
                b_z(2, k, s, 2).start()

    def send_w(k):
        for s in sides_of(k):
            for d in (1, 3):
                w_y(k, s, d, further=d == (3 if s else 1)).start()

    def relay_w(k):
        for s in (0, 1) if 0 < k < 8 else (0,):
            d = 3 if s else 1
            w_y(k, s, d, further=True).wait_recv()
            w_y(k, s, d, d).start()

    def step_b(k):
        sides = (0, 1) if k < 8 else (0,)
        for part in (0, 1):
            for s in sides:
                b_z(part, k - 1, s, 1).wait_recv()
                if k + 2 <= (7 if s else 8):
                    b_z(part, k, s, 2).start()
                if k >= NEAR and part == 0:
                    for d in (2, 1, 3):
                        s_y(k, s, d).start()
        for s in sides:
            for d in (1, 3):
                b_y(k, s, d, further=d == (3 if s else 1)).start()

    def relay(k):
        for s in (0, 1) if 0 < k < 8 else (0,):
            d = 3 if s else 1
            b_y(k, s, d, further=True).wait_recv()
            b_y(k, s, d, d).start()

    for stage in range(1, 5):
        with jax.named_scope(f"b{stage}"):
            step_b(2 * stage - 1)
            step_b(2 * stage)
        work(2 * stage - 1)
        work(2 * stage)
        with jax.named_scope(f"relay{stage}"):
            for k in ((), (0,), (1, 2), (3, 4))[stage - 1]:
                relay(k)
        with jax.named_scope(f"w{stage}"):
            for k in ((), (1, 2), (3, 4), (5, 6))[stage - 1]:
                step_w(k)
    for d in FAR_FIRST:
        t_copy(d).start()
    with jax.named_scope("relay58"):
        for k in (5, 6, 7, 8):
            relay(k)
    for k in range(7):
        send_w(k)
    h_copy.wait_recv()
    before = ht[...].astype(F32)
    nb[ROWS:, :] = normalized(jnp.concatenate([before, before], axis=0))
    take(wb.at[0:9, 0:2, 0:4], by_r.at[0])
    take(wb.at[0:7, 0:3, 0], by_r.at[1])

    def w_b(w, first=0, count=NZ):
        return wb[first : first + count, :, w].reshape(count * 128, CH)

    def project(w, rows=ROWS):
        return jnp.dot(nb[0:rows, :], w, preferred_element_type=F32).astype(BF16)

    state_in = project(w_b(0))
    perm = jnp.where(interleave, 1.0, 0.0).astype(BF16)
    xp = jnp.dot(perm, state_in, preferred_element_type=F32)
    xp_s[...] = xp
    drive = jnp.dot(xp.astype(BF16), coup[...], preferred_element_type=F32)
    v_re, v_im = drive[:, :FLAT], drive[:, FLAT:]
    a_re, a_im = prm[2:3, :], prm[3:4, :]
    dr[...] = v_re * a_re - v_im * a_im
    di[...] = v_re * a_im + v_im * a_re

    def advance(j, h):
        rows = pl.ds(pl.multiple_of(j * 8, 8), 8)
        b_re, b_im, d_re, d_im = br[rows, :], bi[rows, :], dr[rows, :], di[rows, :]
        re, im = h[0] + d_re, h[1] + d_im
        return (b_re * re - b_im * im - d_re, b_re * im + b_im * re - d_im)

    zero = jnp.zeros((8, FLAT), F32)
    end_re, end_im = lax.fori_loop(0, 32, advance, (zero, zero))
    ec[0] = end_re
    ec[1] = end_im

    def chain(re, im, keep):
        for c in range(8):
            if keep:
                hc[0, c : c + 1, :] = re
                hc[1, c : c + 1, :] = im
            p_re, p_im = pc[0, c : c + 1, :], pc[1, c : c + 1, :]
            re, im = (p_re * re - p_im * im + ec[0, c : c + 1, :], p_re * im + p_im * re + ec[1, c : c + 1, :])
        return re, im

    none = jnp.zeros((1, FLAT), F32)
    e_re, e_im = chain(none, none, False)
    for i in range(4):
        ends[z, i : i + 1, :] = e_re[:, i * 128 : (i + 1) * 128]
        ends[z, 4 + i : 5 + i, :] = e_im[:, i * 128 : (i + 1) * 128]

    def e_copy(d):
        return pltpu.make_async_remote_copy(
            ends.at[z], ends.at[z], e_s, e_r,
            device_id=(lax.rem(z + d, NZ), y, t), device_id_type=MESH)

    for d in FAR_FIRST:
        e_copy(d).start()

    for k in (7, 8):
        step_w(k)
        send_w(k)
    take(wb.at[0:7, 0:2, 0:3], by_r.at[2])
    value = project(w_b(1), ROWS + 16).astype(F32)
    inner = project(w_b(2), ROWS + 16).astype(F32)
    gated = (inner * value).astype(BF16).astype(F32)
    ext[8 : 8 + ROWS, :] = gated[:ROWS]
    ext[0:8, :] = jnp.where(z == 0, 0.0, gated[ROWS : ROWS + 8])
    with jax.named_scope("relay_w04"):
        for k in (0, 1, 2, 3, 4):
            relay_w(k)
    outer = project(w_b(3)).astype(F32)
    for k in (5, 6, 7, 8):
        relay_w(k)
    take(ring_t.at[0:15], tz_r)
    powers = [complex_power(ring_t[j], pk[0, 0:4, :], pk[1, 0:4, :]) for j in range(NZ)]
    filtered = taps[0:1, :] * ext[6 : 6 + ROWS, :] + taps[1:2, :] * ext[7 : 7 + ROWS, :] + taps[2:3, :] * ext[8 : 8 + ROWS, :]
    mix[:, CH:] = (outer * filtered).astype(BF16)

    take(ends.at[0:15], e_r)
    re, im = pk[4, 0:4, :], pk[5, 0:4, :]
    in_re, in_im = re, im
    for j in range(NZ):
        p_re, p_im = powers[j]
        re, im = (p_re * re - p_im * im + ends[j, 0:4, :], p_re * im + p_im * re + ends[j, 4:8, :])
        if j < NZ - 1:
            here = z == j + 1
            in_re, in_im = jnp.where(here, re, in_re), jnp.where(here, im, in_im)
    rows8[0, 0:4, :] = in_re
    rows8[0, 4:8, :] = in_im
    rows8[1, 0:4, :] = re
    rows8[1, 4:8, :] = im

    def as_line(n, at):
        return jnp.concatenate([rows8[n, at + i : at + i + 1, :] for i in range(4)], axis=1)

    chain(as_line(0, 0), as_line(0, 4), True)

    def advance2(i, h):
        one = advance(2 * i, h)
        two = advance(2 * i + 1, one)
        rows = pl.ds(pl.multiple_of(i * 16, 16), 16)
        hd[rows, :FLAT] = jnp.concatenate([one[0], two[0]], axis=0).astype(BF16)
        hd[rows, FLAT:] = jnp.concatenate([one[1], two[1]], axis=0).astype(BF16)
        return two

    lax.fori_loop(0, 16, advance2, (hc[0], hc[1]))
    skip_w = jnp.dot(skip[...], ((iota((16, CH), 1) & 15) == iota((16, CH), 0)).astype(F32), precision=HIGHEST, preferred_element_type=F32)
    skip_l = jnp.sum(jnp.where((iota((8, CH), 1) >> 4) == iota((8, CH), 0), skip_w, 0.0), axis=0, keepdims=True)
    v = lax.dot_general(hd[...], readw[...], NT, preferred_element_type=F32) + skip_l * xp_s[...]
    smix = (0.5 * v * (1.0 + jnp.tanh(0.7978845608028654 * (v + 0.044715 * (v * v * v))))).astype(BF16)
    back = jnp.where(col == (row & 31) * 8 + (row >> 5), 1.0, 0.0).astype(BF16)
    mix[:, :CH] = jnp.dot(back, smix, preferred_element_type=F32).astype(BF16)

    def rows_of(core):
        return jnp.concatenate([mix[pl.ds(pl.multiple_of(b * 64 + core * 32, 32), 32), :] for b in range(NX)], axis=0)

    def w_out(n):
        return jnp.concatenate([w_b(4, n * NZ // NCHUNK, NZ // NCHUNK), w_b(5, n * NZ // NCHUNK, NZ // NCHUNK)], axis=1)

    def p_copy(n):
        return pltpu.make_async_remote_copy(
            ps.at[n], pr.at[n], p_s, p_r.at[n], device_id=(z, y, xx * 2 + other), device_id_type=MESH)

    def x_copy(n, kind):
        up = 1 if n % 2 == 0 else NX - 1
        d = up if kind < 2 else NX - up
        src = (cs.at[n, lax.rem(xx + 2, NX)], rl.at[n, 1], cs.at[n, lax.rem(xx + NX - up, NX)])[kind]
        dst = (rl.at[n, 0], rb.at[n, 0], rb.at[n, 1])[kind]
        return pltpu.make_async_remote_copy(
            src, dst, x_s, x_r.at[min(kind, 1), n],
            device_id=(z, y, lax.rem(xx + d, NX) * 2 + cc), device_id_type=MESH)

    take(wb.at[:, :, 0], by_r.at[3])
    theirs, ours = rows_of(other), rows_of(cc)
    for n in range(NCHUNK):
        ps[n] = lax.dot_general(theirs, w_out(n), NT, preferred_element_type=F32).astype(BF16)
        p_copy(n).start()
    for n in range(NCHUNK):
        part = lax.dot_general(ours, w_out(n), NT, preferred_element_type=F32)
        p_copy(n).wait_recv()
        cs[n] = (part + pr[n].astype(F32)).astype(BF16).reshape(NX, 32, CW)
        x_copy(n, 0).start()
    for n in range(NCHUNK):
        x_copy(n, 2).start()
    far = jnp.where(own, jnp.broadcast_to(as_line(1, 0), (8, FLAT)), 0.0)
    far_i = jnp.where(own, jnp.broadcast_to(as_line(1, 4), (8, FLAT)), 0.0)
    pick = ((iota((4, FLAT), 1) & 63) == z * 4 + iota((4, FLAT), 0)).astype(F32)
    fin[0] = lax.dot_general(pick, far, NT, precision=HIGHEST, preferred_element_type=F32)
    fin[1] = lax.dot_general(pick, far_i, NT, precision=HIGHEST, preferred_element_type=F32)
    for n in range(NCHUNK):
        to = lax.rem(xx + (1 if n % 2 == 0 else NX - 1), NX)
        x_copy(n, 0).wait_recv()
        rl[n, 1] = (rl[n, 0].astype(F32) + cs[n, to].astype(F32)).astype(BF16)
        x_copy(n, 1).start()
    for n in range(NCHUNK):
        take(rb.at[n], x_r.at[1, n])
        total = cs[n, xx].astype(F32) + rb[n, 0].astype(F32) + rb[n, 1].astype(F32)
        out[:, n * CW : (n + 1) * CW] = total.astype(BF16)

    take(wb.at[0:12], by_s)
    take(wb.at[0:15, 0], bz_s)
    h_copy.wait_send()
    take(ring_t.at[0:15], tz_s)
    take(ends.at[0:15], e_s)
    take(ps, p_s)
    take(cs.at[0:3], x_s)


def body(
    tokens, norm_gain, w_state_in, w_value, w_outer, w_inner, w_state_out, w_conv_out, log_step, decay_real, frequency,
    step_rate, input_real, input_imag, read_real, read_imag, skip_gain, conv_taps, initial_state,
):
    small = (
        norm_gain.reshape(1, D), log_step.reshape(1, 8), decay_real, frequency, step_rate,
        input_real.transpose(0, 2, 1).reshape(CH, 64), input_imag.transpose(0, 2, 1).reshape(CH, 64), read_real.reshape(CH, 64), read_imag.reshape(CH, 64), skip_gain, conv_taps,
        initial_state.reshape(16, 64),
    )
    dma = pltpu.SemaphoreType.DMA
    anywhere = pl.BlockSpec(memory_space=pl.ANY)
    vmem = pl.BlockSpec(memory_space=pltpu.VMEM)
    mixed, final = pl.pallas_call(
        layer_kernel,
        name="layer",
        out_shape=(pltpu.VMEM((32, D), BF16), pltpu.VMEM((2, 4, 8), F32)),
        in_specs=[anywhere] * (7 + len(small)),
        out_specs=(vmem, vmem),
        scratch_shapes=[pltpu.VMEM(a.shape, a.dtype) for a in small]
        + [
            pltpu.VMEM((NZ, NY, 6, 32, CH), BF16),
            pltpu.VMEM((ROWS, D), BF16),
            pltpu.VMEM((ROWS + 16, D), BF16),
            pltpu.VMEM((8, FLAT), F32),
            pltpu.VMEM((6, 8, 128), F32),
            pltpu.VMEM((ROWS, 128), F32),
            pltpu.VMEM((8, 128), F32),
            pltpu.VMEM((NZ, 1, 128), F32),
            pltpu.VMEM((ROWS, FLAT), F32),
            pltpu.VMEM((ROWS, FLAT), F32),
            pltpu.VMEM((2, 8, FLAT), F32),
            pltpu.VMEM((ROWS, FLAT), F32),
            pltpu.VMEM((ROWS, FLAT), F32),
            pltpu.VMEM((CH, 2 * FLAT), BF16),
            pltpu.VMEM((CH, 2 * FLAT), BF16),
            pltpu.VMEM((ROWS, CH), F32),
            pltpu.VMEM((8 + ROWS, CH), F32),
            pltpu.VMEM((8, D), BF16),
            pltpu.VMEM((NZ, 8, 128), F32),
            pltpu.VMEM((2, 8, FLAT), F32),
            pltpu.VMEM((2, 8, FLAT), F32),
            pltpu.VMEM((2, 8, 128), F32),
            pltpu.VMEM((ROWS, 2 * FLAT), BF16),
            pltpu.VMEM((ROWS, 2 * CH), BF16),
            pltpu.VMEM((NCHUNK, 128, CW), BF16),
            pltpu.VMEM((NCHUNK, 128, CW), BF16),
            pltpu.VMEM((NCHUNK, NX, 32, CW), BF16),
            pltpu.VMEM((NCHUNK, 2, 32, CW), BF16),
            pltpu.VMEM((NCHUNK, 2, 32, CW), BF16),
            dma((len(small),)),
            dma,
            dma,
            dma, dma((3, 2, 8)),
            dma, dma((4,)), dma((NZ,)), dma((NZ,)),
            dma, dma,
            dma, dma,
            dma, dma,
            dma, dma((NCHUNK,)),
            dma, dma((2, NCHUNK)),
        ],
        compiler_params=pltpu.CompilerParams(collective_id=0, has_side_effects=True),
    )(tokens.reshape(ROWS, D), w_state_in, w_value, w_inner, w_outer, w_state_out, w_conv_out, *small)
    return (mixed.reshape(1, 32, D), final.transpose(0, 2, 1).reshape(1, 2, 8, 4))


def solution(mesh):
    return jax.shard_map(
        body,
        mesh=mesh,
        in_specs=(
            P("fs", "sp", None),
            P(),
            P(("sp", "fs"), "tp"),
            P(("sp", "fs"), "tp"),
            P(("sp", "fs"), "tp"),
            P(("sp", "fs"), "tp"),
            P(("sp", "fs"), "tp"),
            P(("sp", "fs"), "tp"),
            P("tp"),
            P("tp", None),
            P("tp", None),
            P("fs", "sp"),
            P("tp", None, None),
            P("tp", None, None),
            P("tp", None, None),
            P("tp", None, None),
            P("tp", None),
            P(None, "tp"),
            P("fs", None, "tp", None),
        ),
        out_specs=(P("fs", ("sp", "tp"), None), P("fs", None, "tp", "sp")),
        check_vma=False,
    )
```

profile of v0, /device:TPU:1, one launch (start us, length us, event | category | flops | bytes accessed | tf_op | source)
XLA Modules:
  0.0 59.9 jit_solution(2635317527546041770)
XLA Ops:
  0.6 58.0 %layer.1 = (bf16[32,2048]{1,0:T(8,128)(2,1)S(1)}, f32[2,4,8]{2,1,0:T(4,128)S(1)}) custom-call(bf16[256,2048]{1,0:T(8,128)(2,1)} %bitcast.18, bf16[32,128]{1,0:T(8,128)(2,1)} %refs_1_.1, bf16[32,128]{1,0:T(8,128)(2,1)} %refs_2_.1, bf16[32,128]{1,0:T(8,128)(2,1)} %refs_3_.1, bf16[32,128]{1,0:T(8,128)(2,1)} %refs_4_.1, bf16[32,128]{1,0:T(8,128)(2,1)} %refs_5_.1, ...), custom_call_target="tpu_custom_call" | custom-call | tf_op jit(solution)/shard_map/layer/pallas_call | solution.py:430
  58.6 0.7 %copy.23 = bf16[1,32,2048]{2,1,0:T(8,128)(2,1)} copy(bf16[1,32,2048]{2,1,0:T(8,128)(2,1)S(1)} %bitcast.16) | data formatting | bytes 262144
  59.3 0.6 copy.24
where the time goes:
time: 60 us; the launch traced here: 59.9 us
  Pallas kernels  58 us (97%)
  local copies, waits for them, and re-layouts  1.25 us (2%)
  between operations  0.65 us (1%)
    pallas_call x1, Pallas kernels, body(): pl.pallas_call(layer_kernel, name='layer', out_shape=(pltpu.VMEM((32, D),...  58 us
    unnamed x2, local copies, waits for them, and re-layouts  1.25 us

commit v1 on v0

--- a/solution.py
+++ b/solution.py
@@ -15,7 +15,7 @@
 NT = (((1,), (1,)), ((), ()))
 NCHUNK = 4
 CW = D // NCHUNK
-NEAR = 5
+NEAR = 3
 FAR_FIRST = (8, 7, 9, 6, 10, 5, 11, 4, 12, 3, 13, 2, 14, 1, 15)
 SIN = [math.pi, -(math.pi**3) / 6, math.pi**5 / 120, -(math.pi**7) / 5040, math.pi**9 / 362880, -(math.pi**11) / 39916800]
 COS = [1.0, -(math.pi**2) / 2, math.pi**4 / 24, -(math.pi**6) / 720, math.pi**8 / 40320, -(math.pi**10) / 3628800, math.pi**12 / 479001600]
@@ -55,9 +55,9 @@
     rest = refs[9 + n_small :]
     small_v = rest[:n_small]
     (
-        wb, tk, nb, prm, pk, ratep, tchunk, ring_t, br, bi, pc, dr, di, coup, readw, xp_s, ext, ht,
-        ends, ec, hc, rows8, hd, mix, ps, pr, cs, rl, rb,
-        ssem, lsem, tsem, bz_s, bz_r, by_s, by_r, br_r, bw_r, tz_s, tz_r, h_s, h_r, e_s, e_r,
+        wa, wb, tk, nb, nbp, prm, pk, ratep, tchunk, ring_t, br, bi, pc, dr, di, coup, readw, xp_s, ext, ht,
+        ends, ec, hc, rows8, hd, way_back, mix, ps, pr, cs, rl, rb,
+        ssem, lsem, tsem, ya_s, ya_r, az_s, az_r, bz_s, bz_r, by_s, by_r, br_r, bw_r, tz_s, tz_r, h_s, h_r, e_s, e_r,
         p_s, p_r, x_s, x_r,
     ) = rest[n_small:]
     gain, lstep, decay, freq, rate, in_r, in_i, rd_r, rd_i, skip, taps, init = small_v
@@ -81,7 +81,9 @@
     def take(ref, sem):
         pltpu.make_async_copy(ref, ref, sem).wait()
 
-    local = [pltpu.make_async_copy(shards[w], wb.at[z, y, w], lsem) for w in range(6)]
+    local = [pltpu.make_async_copy(shards[w], wb.at[z, y, w], lsem) for w in range(5)]
+    mine = pl.ds(pl.multiple_of(z * 128 + y * 32, 32), 32)
+    local.append(pltpu.make_async_copy(shards[5], wa.at[mine, :], lsem))
     tok = pltpu.make_async_copy(tokens, tk, tsem)
     for c in local:
         c.start()
@@ -89,13 +91,34 @@
         c.start()
     tok.start()
     pl.semaphore_wait(barrier, 10)
-    take(wb.at[0, 0], lsem)
+    take(wb.at[0, 0:2, 0:3], lsem)
+
+    def sides_of(k):
+        return (0, 1) if 0 < k < 8 else (0,)
 
     def at_distance(k, side):
         return lax.rem(z + (k if side else NZ - k), NZ)
 
+    def a_y(d):
+        return pltpu.make_async_remote_copy(
+            wa.at[mine, :], wa.at[mine, :], ya_s, ya_r, device_id=(z, lax.rem(y + d, NY), t), device_id_type=MESH)
+
+    def a_z(k, side, part=None):
+        at = at_distance(k, side) * 128
+        rows = pl.ds(pl.multiple_of(at, 128), 128)
+        if part is not None:
+            rows = pl.ds(pl.multiple_of(at + part * 64, 64), 64)
+        return pltpu.make_async_remote_copy(
+            wa.at[rows, :], wa.at[rows, :], az_s, az_r.at[side, k],
+            device_id=(at_distance(1, 1 - side), y, t), device_id_type=MESH)
+
+    def step_a(k, last=False):
+        for s in (0, 1):
+            a_z(k - 1, s).wait_recv()
+            a_z(k, s, s if last else None).start()
+
     def of_part(rows, part):
-        return rows.at[0] if part == 0 else rows.at[pl.ds(1, 3)] if part == 1 else rows.at[pl.ds(4, 2)]
+        return rows.at[0] if part == 0 else rows.at[pl.ds(1, 3)] if part == 1 else rows.at[pl.ds(4, 1)]
 
     def b_z(part, k, side, hop):
         rows = of_part(wb.at[at_distance(k, side), y], part)
@@ -131,6 +154,8 @@
         for hop in (2, 1):
             for side in (0, 1):
                 b_z(part, 0, side, hop).start()
+    for d in (2, 1, 3):
+        a_y(d).start()
     b_y(0, 0, 1, further=True).start()
     b_y(0, 0, 3).start()
 
@@ -144,6 +169,9 @@
     tchunk[...] = totals
     ring_t[z] = jnp.sum(totals, axis=0, keepdims=True)
 
+    take(wb.at[0, 0, 0:3], ya_r)
+    for side in (0, 1):
+        a_z(0, side).start()
     h_copy = pltpu.make_async_remote_copy(
         tokens.at[pl.ds(ROWS - 8, 8), :], ht, h_s, h_r, device_id=(zn, y, t), device_id_type=MESH)
     h_copy.start()
@@ -190,9 +218,6 @@
             br[rows, :] = re
             bi[rows, :] = im
 
-    def sides_of(k):
-        return (0, 1) if 0 < k < 8 else (0,)
-
     def step_w(k):
         for s in sides_of(k):
             b_z(2, k - 1, s, 1).wait_recv()
@@ -210,19 +235,22 @@
             w_y(k, s, d, further=True).wait_recv()
             w_y(k, s, d, d).start()
 
-    def step_b(k):
-        sides = (0, 1) if k < 8 else (0,)
+    def step_b(pair, between):
         for part in (0, 1):
-            for s in sides:
-                b_z(part, k - 1, s, 1).wait_recv()
-                if k + 2 <= (7 if s else 8):
-                    b_z(part, k, s, 2).start()
-                if k >= NEAR and part == 0:
-                    for d in (2, 1, 3):
-                        s_y(k, s, d).start()
-        for s in sides:
-            for d in (1, 3):
-                b_y(k, s, d, further=d == (3 if s else 1)).start()
+            for k in pair:
+                for s in sides_of(k):
+                    b_z(part, k - 1, s, 1).wait_recv()
+                    if k + 2 <= (7 if s else 8):
+                        b_z(part, k, s, 2).start()
+                    if k >= NEAR and part == 0:
+                        for d in (2, 1, 3):
+                            s_y(k, s, d).start()
+            if part == 0 and between:
+                step_a(between)
+        for k in pair:
+            for s in sides_of(k):
+                for d in (1, 3):
+                    b_y(k, s, d, further=d == (3 if s else 1)).start()
 
     def relay(k):
         for s in (0, 1) if 0 < k < 8 else (0,):
@@ -232,8 +260,7 @@
 
     for stage in range(1, 5):
         with jax.named_scope(f"b{stage}"):
-            step_b(2 * stage - 1)
-            step_b(2 * stage)
+            step_b((2 * stage - 1, 2 * stage), stage if stage > 1 else None)
         work(2 * stage - 1)
         work(2 * stage)
         with jax.named_scope(f"relay{stage}"):
@@ -242,18 +269,25 @@
         with jax.named_scope(f"w{stage}"):
             for k in ((), (1, 2), (3, 4), (5, 6))[stage - 1]:
                 step_w(k)
+        if stage == 1:
+            step_a(1)
+    perm = jnp.where(interleave, 1.0, 0.0).astype(BF16)
+    for n in range(0, D, 512):
+        nbp[:, n : n + 512] = jnp.dot(perm, nb[0:ROWS, n : n + 512], preferred_element_type=F32).astype(BF16)
     for d in FAR_FIRST:
         t_copy(d).start()
     with jax.named_scope("relay58"):
-        for k in (5, 6, 7, 8):
+        for k in (5, 6):
             relay(k)
-    for k in range(7):
+    for k in (0, 1, 2):
         send_w(k)
+    with jax.named_scope("a5"):
+        step_a(5)
     h_copy.wait_recv()
     before = ht[...].astype(F32)
     nb[ROWS:, :] = normalized(jnp.concatenate([before, before], axis=0))
-    take(wb.at[0:9, 0:2, 0:4], by_r.at[0])
-    take(wb.at[0:7, 0:3, 0], by_r.at[1])
+    take(wb.at[0:5, 0:2, 0:4], by_r.at[0])
+    take(wb.at[0:11, 0:3, 0], by_r.at[1])
 
     def w_b(w, first=0, count=NZ):
         return wb[first : first + count, :, w].reshape(count * 128, CH)
@@ -261,11 +295,9 @@
     def project(w, rows=ROWS):
         return jnp.dot(nb[0:rows, :], w, preferred_element_type=F32).astype(BF16)
 
-    state_in = project(w_b(0))
-    perm = jnp.where(interleave, 1.0, 0.0).astype(BF16)
-    xp = jnp.dot(perm, state_in, preferred_element_type=F32)
-    xp_s[...] = xp
-    drive = jnp.dot(xp.astype(BF16), coup[...], preferred_element_type=F32)
+    state_in = jnp.dot(nbp[...], w_b(0), preferred_element_type=F32).astype(BF16)
+    xp_s[...] = state_in.astype(F32)
+    drive = jnp.dot(state_in, coup[...], preferred_element_type=F32)
     v_re, v_im = drive[:, :FLAT], drive[:, FLAT:]
     a_re, a_im = prm[2:3, :], prm[3:4, :]
     dr[...] = v_re * a_re - v_im * a_im
@@ -306,24 +338,39 @@
         e_copy(d).start()
 
     for k in (7, 8):
+        relay(k)
+    for k in (3, 4, 5, 6):
+        send_w(k)
+    with jax.named_scope("a6"):
+        step_a(6)
+    for k in (7, 8):
         step_w(k)
         send_w(k)
-    take(wb.at[0:7, 0:2, 0:3], by_r.at[2])
+    with jax.named_scope("vio_wait"):
+        take(wb.at[0:11, 0:2, 0:3], by_r.at[2])
+    with jax.named_scope("relay_w04"):
+        for k in (0, 1, 2, 3, 4):
+            relay_w(k)
+    with jax.named_scope("a7"):
+        step_a(7, last=True)
     value = project(w_b(1), ROWS + 16).astype(F32)
     inner = project(w_b(2), ROWS + 16).astype(F32)
     gated = (inner * value).astype(BF16).astype(F32)
     ext[8 : 8 + ROWS, :] = gated[:ROWS]
     ext[0:8, :] = jnp.where(z == 0, 0.0, gated[ROWS : ROWS + 8])
-    with jax.named_scope("relay_w04"):
-        for k in (0, 1, 2, 3, 4):
+    with jax.named_scope("relay_w58"):
+        for k in (5, 6, 7, 8):
             relay_w(k)
     outer = project(w_b(3)).astype(F32)
-    for k in (5, 6, 7, 8):
-        relay_w(k)
     take(ring_t.at[0:15], tz_r)
     powers = [complex_power(ring_t[j], pk[0, 0:4, :], pk[1, 0:4, :]) for j in range(NZ)]
     filtered = taps[0:1, :] * ext[6 : 6 + ROWS, :] + taps[1:2, :] * ext[7 : 7 + ROWS, :] + taps[2:3, :] * ext[8 : 8 + ROWS, :]
     mix[:, CH:] = (outer * filtered).astype(BF16)
+
+    skip_w = jnp.dot(skip[...], ((iota((16, CH), 1) & 15) == iota((16, CH), 0)).astype(F32), precision=HIGHEST, preferred_element_type=F32)
+    skip_l = jnp.sum(jnp.where((iota((8, CH), 1) >> 4) == iota((8, CH), 0), skip_w, 0.0), axis=0, keepdims=True)
+    direct = skip_l * xp_s[...]
+    way_back[...] = jnp.where(col == (row & 31) * 8 + (row >> 5), 1.0, 0.0).astype(BF16)
 
     take(ends.at[0:15], e_r)
     re, im = pk[4, 0:4, :], pk[5, 0:4, :]
@@ -353,18 +400,15 @@
         return two
 
     lax.fori_loop(0, 16, advance2, (hc[0], hc[1]))
-    skip_w = jnp.dot(skip[...], ((iota((16, CH), 1) & 15) == iota((16, CH), 0)).astype(F32), precision=HIGHEST, preferred_element_type=F32)
-    skip_l = jnp.sum(jnp.where((iota((8, CH), 1) >> 4) == iota((8, CH), 0), skip_w, 0.0), axis=0, keepdims=True)
-    v = lax.dot_general(hd[...], readw[...], NT, preferred_element_type=F32) + skip_l * xp_s[...]
+    v = lax.dot_general(hd[...], readw[...], NT, preferred_element_type=F32) + direct
     smix = (0.5 * v * (1.0 + jnp.tanh(0.7978845608028654 * (v + 0.044715 * (v * v * v))))).astype(BF16)
-    back = jnp.where(col == (row & 31) * 8 + (row >> 5), 1.0, 0.0).astype(BF16)
-    mix[:, :CH] = jnp.dot(back, smix, preferred_element_type=F32).astype(BF16)
+    mix[:, :CH] = jnp.dot(way_back[...], smix, preferred_element_type=F32).astype(BF16)
 
     def rows_of(core):
         return jnp.concatenate([mix[pl.ds(pl.multiple_of(b * 64 + core * 32, 32), 32), :] for b in range(NX)], axis=0)
 
     def w_out(n):
-        return jnp.concatenate([w_b(4, n * NZ // NCHUNK, NZ // NCHUNK), w_b(5, n * NZ // NCHUNK, NZ // NCHUNK)], axis=1)
+        return jnp.concatenate([w_b(4, n * NZ // NCHUNK, 2 * NZ // NCHUNK), wa[n * CW : (n + 2) * CW, :]], axis=1)
 
     def p_copy(n):
         return pltpu.make_async_remote_copy(
@@ -379,16 +423,24 @@
             src, dst, x_s, x_r.at[min(kind, 1), n],
             device_id=(z, y, lax.rem(xx + d, NX) * 2 + cc), device_id_type=MESH)
 
-    take(wb.at[:, :, 0], by_r.at[3])
+    with jax.named_scope("w_wait"):
+        take(wb.at[:, 0:2, 0], by_r.at[3])
+    with jax.named_scope("a8"):
+        for s in (0, 1):
+            a_z(7, s, s).wait_recv()
     theirs, ours = rows_of(other), rows_of(cc)
-    for n in range(NCHUNK):
-        ps[n] = lax.dot_general(theirs, w_out(n), NT, preferred_element_type=F32).astype(BF16)
-        p_copy(n).start()
-    for n in range(NCHUNK):
-        part = lax.dot_general(ours, w_out(n), NT, preferred_element_type=F32)
-        p_copy(n).wait_recv()
-        cs[n] = (part + pr[n].astype(F32)).astype(BF16).reshape(NX, 32, CW)
-        x_copy(n, 0).start()
+    for m in range(0, NCHUNK, 2):
+        both = lax.dot_general(theirs, w_out(m), NT, preferred_element_type=F32).astype(BF16)
+        for n in (m, m + 1):
+            ps[n] = both[:, (n - m) * CW : (n - m + 1) * CW]
+            p_copy(n).start()
+    for m in range(0, NCHUNK, 2):
+        both = lax.dot_general(ours, w_out(m), NT, preferred_element_type=F32)
+        for n in (m, m + 1):
+            p_copy(n).wait_recv()
+            part = both[:, (n - m) * CW : (n - m + 1) * CW]
+            cs[n] = (part + pr[n].astype(F32)).astype(BF16).reshape(NX, 32, CW)
+            x_copy(n, 0).start()
     for n in range(NCHUNK):
         x_copy(n, 2).start()
     far = jnp.where(own, jnp.broadcast_to(as_line(1, 0), (8, FLAT)), 0.0)
@@ -406,6 +458,8 @@
         total = cs[n, xx].astype(F32) + rb[n, 0].astype(F32) + rb[n, 1].astype(F32)
         out[:, n * CW : (n + 1) * CW] = total.astype(BF16)
 
+    take(wb.at[0, 0, 0:3], ya_s)
+    take(wa.at[0:1920, :], az_s)
     take(wb.at[0:12], by_s)
     take(wb.at[0:15, 0], bz_s)
     h_copy.wait_send()
@@ -435,9 +489,11 @@
         out_specs=(vmem, vmem),
         scratch_shapes=[pltpu.VMEM(a.shape, a.dtype) for a in small]
         + [
-            pltpu.VMEM((NZ, NY, 6, 32, CH), BF16),
+            pltpu.VMEM((D, CH), BF16),
+            pltpu.VMEM((NZ, NY, 5, 32, CH), BF16),
             pltpu.VMEM((ROWS, D), BF16),
             pltpu.VMEM((ROWS + 16, D), BF16),
+            pltpu.VMEM((ROWS, D), BF16),
             pltpu.VMEM((8, FLAT), F32),
             pltpu.VMEM((6, 8, 128), F32),
             pltpu.VMEM((ROWS, 128), F32),
@@ -458,6 +514,7 @@
             pltpu.VMEM((2, 8, FLAT), F32),
             pltpu.VMEM((2, 8, 128), F32),
             pltpu.VMEM((ROWS, 2 * FLAT), BF16),
+            pltpu.VMEM((ROWS, ROWS), BF16),
             pltpu.VMEM((ROWS, 2 * CH), BF16),
             pltpu.VMEM((NCHUNK, 128, CW), BF16),
             pltpu.VMEM((NCHUNK, 128, CW), BF16),
@@ -467,6 +524,8 @@
             dma((len(small),)),
             dma,
             dma,
+            dma, dma,
+            dma, dma((2, 8)),
             dma, dma((3, 2, 8)),
             dma, dma((4,)), dma((NZ,)), dma((NZ,)),
             dma, dma,

time: 60 us -> 59.2 us (0.987)
  Pallas kernels: 58 us -> 57.2 us
    pallas_call x1, Pallas kernels: 58 us -> 57.2 us  [body(): pl.pallas_call(layer_kernel, name='layer', out_shape=(pltpu.VMEM((32, D),...]
where the time goes in v1:
time: 59.2 us; the launch traced here: 59.1 us
  Pallas kernels  57.2 us (97%)
  local copies, waits for them, and re-layouts  1.25 us (2%)
  between operations  0.65 us (1%)
    pallas_call x1, Pallas kernels, body(): pl.pallas_call(layer_kernel, name='layer', out_shape=(pltpu.VMEM((32, D),...  57.2 us
    unnamed x2, local copies, waits for them, and re-layouts  1.25 us

profile of v1, /device:TPU:1, one launch (start us, length us, event | category | flops | bytes accessed | tf_op | source)
XLA Modules:
  0.0 59.1 jit_solution(10699258191154589770)
XLA Ops:
  0.6 57.2 %layer.1 = (bf16[32,2048]{1,0:T(8,128)(2,1)S(1)}, f32[2,4,8]{2,1,0:T(4,128)S(1)}) custom-call(bf16[256,2048]{1,0:T(8,128)(2,1)} %bitcast.18, bf16[32,128]{1,0:T(8,128)(2,1)} %refs_1_.1, bf16[32,128]{1,0:T(8,128)(2,1)} %refs_2_.1, bf16[32,128]{1,0:T(8,128)(2,1)} %refs_3_.1, bf16[32,128]{1,0:T(8,128)(2,1)} %refs_4_.1, bf16[32,128]{1,0:T(8,128)(2,1)} %refs_5_.1, ...), custom_call_target="tpu_custom_call" | custom-call | tf_op jit(solution)/shard_map/layer/pallas_call | solution.py:484
  57.9 0.7 %copy.23 = bf16[1,32,2048]{2,1,0:T(8,128)(2,1)} copy(bf16[1,32,2048]{2,1,0:T(8,128)(2,1)S(1)} %bitcast.16) | data formatting | bytes 262144
  58.5 0.6 %copy.24 = f32[1,2,8,4]{2,3,1,0:T(4,128)} copy(f32[1,2,8,4]{2,3,1,0:T(4,128)S(1)} %bitcast.17) | data formatting | bytes 512

commit v2 on v1

--- a/solution.py
+++ b/solution.py
@@ -56,7 +56,7 @@
     small_v = rest[:n_small]
     (
         wa, wb, tk, nb, nbp, prm, pk, ratep, tchunk, ring_t, br, bi, pc, dr, di, coup, readw, xp_s, ext, ht,
-        ends, ec, hc, rows8, hd, way_back, mix, ps, pr, cs, rl, rb,
+        ends, ec, hc, rows8, pw, hd, way_back, mix, ps, pr, cs, rl, rb,
         ssem, lsem, tsem, ya_s, ya_r, az_s, az_r, bz_s, bz_r, by_s, by_r, br_r, bw_r, tz_s, tz_r, h_s, h_r, e_s, e_r,
         p_s, p_r, x_s, x_r,
     ) = rest[n_small:]
@@ -112,10 +112,19 @@
             wa.at[rows, :], wa.at[rows, :], az_s, az_r.at[side, k],
             device_id=(at_distance(1, 1 - side), y, t), device_id_type=MESH)
 
-    def step_a(k, last=False):
+    def a_far(side):
+        rows = pl.ds(pl.multiple_of(at_distance(6, side) * 128 + side * 64, 64), 64)
+        return pltpu.make_async_remote_copy(
+            wa.at[rows, :], wa.at[rows, :], az_s, az_r.at[side, 7],
+            device_id=(at_distance(2, 1 - side), y, t), device_id_type=MESH)
+
+    def step_a(k):
         for s in (0, 1):
             a_z(k - 1, s).wait_recv()
-            a_z(k, s, s if last else None).start()
+            if k < 7:
+                a_z(k, s).start()
+            if k == 6:
+                a_far(s).start()
 
     def of_part(rows, part):
         return rows.at[0] if part == 0 else rows.at[pl.ds(1, 3)] if part == 1 else rows.at[pl.ds(4, 1)]
@@ -226,8 +235,8 @@
 
     def send_w(k):
         for s in sides_of(k):
-            for d in (1, 3):
-                w_y(k, s, d, further=d == (3 if s else 1)).start()
+            for d in (1, 3) if k < 5 else (2, 1, 3):
+                w_y(k, s, d, further=k < 5 and d == (3 if s else 1)).start()
 
     def relay_w(k):
         for s in (0, 1) if 0 < k < 8 else (0,):
@@ -331,7 +340,7 @@
 
     def e_copy(d):
         return pltpu.make_async_remote_copy(
-            ends.at[z], ends.at[z], e_s, e_r,
+            ends.at[z], ends.at[z], e_s, e_r.at[z],
             device_id=(lax.rem(z + d, NZ), y, t), device_id_type=MESH)
 
     for d in FAR_FIRST:
@@ -346,24 +355,23 @@
     for k in (7, 8):
         step_w(k)
         send_w(k)
+    with jax.named_scope("relay_w02"):
+        for k in (0, 1, 2):
+            relay_w(k)
     with jax.named_scope("vio_wait"):
         take(wb.at[0:11, 0:2, 0:3], by_r.at[2])
     with jax.named_scope("relay_w04"):
-        for k in (0, 1, 2, 3, 4):
+        for k in (3, 4):
             relay_w(k)
-    with jax.named_scope("a7"):
-        step_a(7, last=True)
     value = project(w_b(1), ROWS + 16).astype(F32)
     inner = project(w_b(2), ROWS + 16).astype(F32)
     gated = (inner * value).astype(BF16).astype(F32)
     ext[8 : 8 + ROWS, :] = gated[:ROWS]
     ext[0:8, :] = jnp.where(z == 0, 0.0, gated[ROWS : ROWS + 8])
-    with jax.named_scope("relay_w58"):
-        for k in (5, 6, 7, 8):
-            relay_w(k)
     outer = project(w_b(3)).astype(F32)
     take(ring_t.at[0:15], tz_r)
-    powers = [complex_power(ring_t[j], pk[0, 0:4, :], pk[1, 0:4, :]) for j in range(NZ)]
+    for j in range(NZ):
+        pw[j, 0], pw[j, 1] = complex_power(ring_t[j], pk[0, 0:4, :], pk[1, 0:4, :])
     filtered = taps[0:1, :] * ext[6 : 6 + ROWS, :] + taps[1:2, :] * ext[7 : 7 + ROWS, :] + taps[2:3, :] * ext[8 : 8 + ROWS, :]
     mix[:, CH:] = (outer * filtered).astype(BF16)
 
@@ -372,19 +380,16 @@
     direct = skip_l * xp_s[...]
     way_back[...] = jnp.where(col == (row & 31) * 8 + (row >> 5), 1.0, 0.0).astype(BF16)
 
-    take(ends.at[0:15], e_r)
-    re, im = pk[4, 0:4, :], pk[5, 0:4, :]
-    in_re, in_im = re, im
-    for j in range(NZ):
-        p_re, p_im = powers[j]
-        re, im = (p_re * re - p_im * im + ends[j, 0:4, :], p_re * im + p_im * re + ends[j, 4:8, :])
-        if j < NZ - 1:
-            here = z == j + 1
-            in_re, in_im = jnp.where(here, re, in_re), jnp.where(here, im, in_im)
+    def through(j, h):
+        return (pw[j, 0] * h[0] - pw[j, 1] * h[1] + ends[j, 0:4, :], pw[j, 0] * h[1] + pw[j, 1] * h[0] + ends[j, 4:8, :])
+
+    def next_span(j, h):
+        take(ends.at[j], e_r.at[j])
+        return through(j, h)
+
+    in_re, in_im = lax.fori_loop(0, z, next_span, (pk[4, 0:4, :], pk[5, 0:4, :]))
     rows8[0, 0:4, :] = in_re
     rows8[0, 4:8, :] = in_im
-    rows8[1, 0:4, :] = re
-    rows8[1, 4:8, :] = im
 
     def as_line(n, at):
         return jnp.concatenate([rows8[n, at + i : at + i + 1, :] for i in range(4)], axis=1)
@@ -424,8 +429,9 @@
             device_id=(z, y, lax.rem(xx + d, NX) * 2 + cc), device_id_type=MESH)
 
     with jax.named_scope("w_wait"):
-        take(wb.at[:, 0:2, 0], by_r.at[3])
+        take(wb.at[0:13, 0:3, 0], by_r.at[3])
     with jax.named_scope("a8"):
+        step_a(7)
         for s in (0, 1):
             a_z(7, s, s).wait_recv()
     theirs, ours = rows_of(other), rows_of(cc)
@@ -443,6 +449,9 @@
             x_copy(n, 0).start()
     for n in range(NCHUNK):
         x_copy(n, 2).start()
+    re, im = lax.fori_loop(z + 1, NZ, next_span, through(z, (in_re, in_im)))
+    rows8[1, 0:4, :] = re
+    rows8[1, 4:8, :] = im
     far = jnp.where(own, jnp.broadcast_to(as_line(1, 0), (8, FLAT)), 0.0)
     far_i = jnp.where(own, jnp.broadcast_to(as_line(1, 4), (8, FLAT)), 0.0)
     pick = ((iota((4, FLAT), 1) & 63) == z * 4 + iota((4, FLAT), 0)).astype(F32)
@@ -513,6 +522,7 @@
             pltpu.VMEM((2, 8, FLAT), F32),
             pltpu.VMEM((2, 8, FLAT), F32),
             pltpu.VMEM((2, 8, 128), F32),
+            pltpu.VMEM((NZ, 2, 4, 128), F32),
             pltpu.VMEM((ROWS, 2 * FLAT), BF16),
             pltpu.VMEM((ROWS, ROWS), BF16),
             pltpu.VMEM((ROWS, 2 * CH), BF16),
@@ -530,7 +540,7 @@
             dma, dma((4,)), dma((NZ,)), dma((NZ,)),
             dma, dma,
             dma, dma,
-            dma, dma,
+            dma, dma((NZ,)),
             dma, dma((NCHUNK,)),
             dma, dma((2, NCHUNK)),
         ],

time: 59.2 us -> 58.3 us (0.985)
  Pallas kernels: 57.2 us -> 56.2 us
    pallas_call x1, Pallas kernels: 57.2 us -> 56.2 us  [body(): pl.pallas_call(layer_kernel, name='layer', out_shape=(pltpu.VMEM((32, D),...]
where the time goes in v2:
time: 58.3 us; the launch traced here: 58.1 us
  Pallas kernels  56.2 us (96%)
  local copies, waits for them, and re-layouts  1.25 us (2%)
  between operations  0.65 us (1%)
    pallas_call x1, Pallas kernels, body(): pl.pallas_call(layer_kernel, name='layer', out_shape=(pltpu.VMEM((32, D),...  56.2 us
    unnamed x2, local copies, waits for them, and re-layouts  1.25 us

profile of v2, /device:TPU:1, one launch (start us, length us, event | category | flops | bytes accessed | tf_op | source)
XLA Modules:
  0.0 58.1 jit_solution(5673413135360679841)
XLA Ops:
  0.6 56.2 %layer.1 = (bf16[32,2048]{1,0:T(8,128)(2,1)S(1)}, f32[2,4,8]{2,1,0:T(4,128)S(1)}) custom-call(bf16[256,2048]{1,0:T(8,128)(2,1)} %bitcast.18, bf16[32,128]{1,0:T(8,128)(2,1)} %refs_1_.1, bf16[32,128]{1,0:T(8,128)(2,1)} %refs_2_.1, bf16[32,128]{1,0:T(8,128)(2,1)} %refs_3_.1, bf16[32,128]{1,0:T(8,128)(2,1)} %refs_4_.1, bf16[32,128]{1,0:T(8,128)(2,1)} %refs_5_.1, ...), custom_call_target="tpu_custom_call" | custom-call | tf_op jit(solution)/shard_map/layer/pallas_call | solution.py:493
  56.9 0.7 %copy.23 = bf16[1,32,2048]{2,1,0:T(8,128)(2,1)} copy(bf16[1,32,2048]{2,1,0:T(8,128)(2,1)S(1)} %bitcast.16) | data formatting | bytes 262144
  57.5 0.6 %copy.24 = f32[1,2,8,4]{2,3,1,0:T(4,128)} copy(f32[1,2,8,4]{2,3,1,0:T(4,128)S(1)} %bitcast.17) | data formatting | bytes 512
